TPU v7x, 32 devices: a whole 2x2x4 slice. The times are simulated.
32 devices in a mesh: sp: 8 (over z, y), tp: 4 (over x, core).
Axes of the slice: x: 2, y: 2, z: 4, core: 2. Of those that a mesh axis runs over, the one named last changes fastest.
Arguments:
- latent: bfloat16 [4096, 4096], P(('sp', 'tp')), may hold values from -3 to 3
- context: bfloat16 [1024, 4096], P('sp'), may hold values from -6 to 6
- cond: float32 [4096], replicated, may hold values from -6 to 6
- ctx_cond: float32 [4096], replicated, may hold values from -6 to 6
- w_shift: bfloat16 [4096, 4096], P('sp', 'tp'), may hold values from -0.1875 to 0.1875
- w_scale: bfloat16 [4096, 4096], P('sp', 'tp'), may hold values from -0.09375 to 0.15478516
- w_gate: bfloat16 [4096, 4096], P('sp', 'tp'), may hold values from -0.1875 to 0.1875
- w_query: bfloat16 [4096, 2048], P(None, 'tp'), may hold values from -0.09375 to 0.09375
- key_weight: bfloat16 [4096, 1024], P(None, 'tp'), may hold values from -0.09375 to 0.09375
- value_weight: bfloat16 [4096, 1024], P(None, 'tp'), may hold values from -0.09375 to 0.09375
- w_out: bfloat16 [2048, 4096], P('tp'), may hold values from -0.125 to 0.125
- sink: float32 [16], replicated, may hold values from 4 to 8
Outputs:
- mixed: bfloat16 [4096, 4096], P(('sp', 'tp'))
All inputs are finite; a program needn't handle non-finite values.
Results may differ from a plain program's by a relative error of at most 0.035.
Values may be sent and summed in bfloat16 or wider, within the bound.
A program may use at most 64 MiB of HBM per device.

v0:
```python
import jax
import jax.numpy as jnp
from jax import lax
from jax.sharding import PartitionSpec as P

HEAD_SIZE = 128
WINDOW_SIDE = 128
GRID_WIDTH = 64
EPS = 1e-05
THETA = 10000.0
MASKED = -1e30


def with_halo(cells, sides, width):
    for axis, dim in sides:
        count = lax.axis_size(axis)
        ends = count - 1
        head = lax.slice_in_dim(cells, 0, width, axis=dim)
        tail = lax.slice_in_dim(cells, cells.shape[dim] - width, cells.shape[dim], axis=dim)
        cells = jnp.concatenate(
            [
                lax.ppermute(tail, axis, [(i, (i + 1) % count) for i in range(ends)]),
                cells,
                lax.ppermute(head, axis, [((i + 1) % count, i) for i in range(ends)]),
            ],
            axis=dim,
        )
    return cells


def layer_norm(rows):
    values = rows.astype(jnp.float32)
    mean = jnp.mean(values, axis=-1, keepdims=True)
    var = jnp.mean(jnp.square(values - mean), axis=-1, keepdims=True)
    return (values - mean) * lax.rsqrt(var + EPS)


def rotate_half(values, token_position, width):
    half = width // 2
    inverse = THETA ** (-jnp.arange(half, dtype=jnp.float32) * 2.0 / width)
    angle = token_position.astype(jnp.float32)[:, None] * inverse[None, :]
    cosine = jnp.cos(angle)[:, None, :]
    sine = jnp.sin(angle)[:, None, :]
    first = values[..., :half]
    second = values[..., half:]
    return jnp.concatenate(
        [first * cosine - second * sine, second * cosine + first * sine], axis=-1
    )


def axial_rotation(heads, token_position, grid):
    width = heads.shape[-1] // 2
    values = heads.astype(jnp.float32)
    turned = jnp.concatenate(
        [
            rotate_half(values[..., :width], token_position // grid, width),
            rotate_half(values[..., width:], token_position % grid, width),
        ],
        axis=-1,
    )
    return turned.astype(jnp.bfloat16)


def sink_weights(scores, sink_column):
    top = jnp.maximum(jnp.max(scores, axis=-1, keepdims=True), sink_column)
    expo = jnp.exp(scores - top)
    return (expo / (jnp.sum(expo, axis=-1, keepdims=True) + jnp.exp(sink_column - top))).astype(
        jnp.bfloat16
    )


def shards(
    latent,
    context,
    cond,
    ctx_cond,
    w_shift,
    w_scale,
    w_gate,
    w_query,
    key_weight,
    value_weight,
    w_out,
    sink,
):
    sp_count = lax.axis_size("sp")
    sp_index = lax.axis_index("sp")
    tp_index = lax.axis_index("tp")
    block_rows = w_shift.shape[0]
    act = jax.nn.silu(jnp.stack([cond, ctx_cond])).astype(jnp.bfloat16)
    own_act = lax.dynamic_slice_in_dim(act, sp_index * block_rows, block_rows, 1)
    shift_part = jnp.dot(own_act, w_shift, preferred_element_type=jnp.float32)
    scale_part = jnp.dot(own_act, w_scale, preferred_element_type=jnp.float32)
    gate_part = jnp.dot(own_act[0:1], w_gate, preferred_element_type=jnp.float32)
    shift_sum, scale_sum, gate_sum = lax.psum((shift_part, scale_part, gate_part), "sp")
    shift, scale, gate = (
        lax.all_gather(shift_sum, "tp", axis=1, tiled=True),
        lax.all_gather(scale_sum, "tp", axis=1, tiled=True),
        lax.all_gather(gate_sum, "tp", axis=1, tiled=True),
    )
    latent_mod = (layer_norm(latent) * (1.0 + scale[0]) + shift[0]).astype(jnp.bfloat16)
    ctx_mod = (layer_norm(context) * (1.0 + scale[1]) + shift[1]).astype(jnp.bfloat16)
    kv_cols = key_weight.shape[1]
    q_cols = w_query.shape[1]
    ctx_pair = lax.all_gather(
        jnp.concatenate(
            [
                jnp.dot(ctx_mod, key_weight, preferred_element_type=jnp.float32).astype(
                    jnp.bfloat16
                ),
                jnp.dot(ctx_mod, value_weight, preferred_element_type=jnp.float32).astype(
                    jnp.bfloat16
                ),
            ],
            axis=1,
        ),
        "sp",
        axis=0,
        tiled=True,
    )
    piece = lax.all_gather(latent_mod, "tp", axis=0, tiled=True)
    projected_rows = jnp.concatenate(
        [
            jnp.dot(piece, w_query, preferred_element_type=jnp.float32).astype(jnp.bfloat16),
            jnp.dot(piece, key_weight, preferred_element_type=jnp.float32).astype(jnp.bfloat16),
            jnp.dot(piece, value_weight, preferred_element_type=jnp.float32).astype(jnp.bfloat16),
        ],
        axis=1,
    )
    tokens_here = projected_rows.shape[0]
    kv_heads = kv_cols // HEAD_SIZE
    q_heads = q_cols // HEAD_SIZE
    query_group = q_heads // kv_heads
    offset = sp_index * tokens_here
    token_position = offset + jnp.arange(tokens_here, dtype=jnp.int32)
    query = axial_rotation(
        projected_rows[:, :q_cols].reshape(tokens_here, q_heads, HEAD_SIZE),
        token_position,
        GRID_WIDTH,
    )
    key = axial_rotation(
        projected_rows[:, q_cols : q_cols + kv_cols].reshape(tokens_here, kv_heads, HEAD_SIZE),
        token_position,
        GRID_WIDTH,
    )
    value_rows = projected_rows[:, q_cols + kv_cols :]
    extended = with_halo(
        jnp.concatenate([key.reshape(tokens_here, kv_cols), value_rows], axis=1),
        (("sp", 0),),
        WINDOW_SIDE,
    )
    block_list = tokens_here // WINDOW_SIDE
    band = jnp.concatenate(
        [
            extended[shift_index * WINDOW_SIDE : shift_index * WINDOW_SIDE + tokens_here].reshape(
                block_list, WINDOW_SIDE, 2 * kv_cols
            )
            for shift_index in range(3)
        ],
        axis=1,
    )
    band_key = band[..., :kv_cols].reshape(block_list, 3 * WINDOW_SIDE, kv_heads, HEAD_SIZE)
    band_value = band[..., kv_cols:].reshape(block_list, 3 * WINDOW_SIDE, kv_heads, HEAD_SIZE)
    context_key_rows = ctx_pair[:, :kv_cols].reshape(-1, kv_heads, HEAD_SIZE)
    context_value_rows = ctx_pair[:, kv_cols:].reshape(-1, kv_heads, HEAD_SIZE)
    query_block_list = query.reshape(block_list, WINDOW_SIDE, kv_heads, query_group, HEAD_SIZE)
    factor = HEAD_SIZE ** (-0.5)
    band_scores = (
        jnp.einsum(
            "nqhgd,nkhd->nhgqk", query_block_list, band_key, preferred_element_type=jnp.float32
        )
        * factor
    )
    total = tokens_here * sp_count
    qpos = token_position.reshape(block_list, WINDOW_SIDE)[:, :, None]
    kpos = (
        offset
        - WINDOW_SIDE
        + (jnp.arange(block_list, dtype=jnp.int32) * WINDOW_SIDE)[:, None, None]
        + jnp.arange(3 * WINDOW_SIDE, dtype=jnp.int32)[None, None, :]
    )
    valid = (jnp.abs(kpos - qpos) <= WINDOW_SIDE) & (kpos >= 0) & (kpos < total)
    band_scores = jnp.where(valid[:, None, None], band_scores, MASKED)
    ctx_scores = (
        jnp.einsum(
            "nqhgd,khd->nhgqk",
            query_block_list,
            context_key_rows,
            preferred_element_type=jnp.float32,
        )
        * factor
    )
    own_sink = lax.dynamic_slice_in_dim(sink, tp_index * q_heads, q_heads).reshape(
        kv_heads, query_group
    )[:, :, None, None]
    weights = sink_weights(jnp.concatenate([band_scores, ctx_scores], axis=-1), own_sink)
    attended = jnp.einsum(
        "nhgqk,nkhd->nqhgd",
        weights[..., : 3 * WINDOW_SIDE],
        band_value,
        preferred_element_type=jnp.float32,
    ) + jnp.einsum(
        "nhgqk,khd->nqhgd",
        weights[..., 3 * WINDOW_SIDE :],
        context_value_rows,
        preferred_element_type=jnp.float32,
    )
    attended = attended.astype(jnp.bfloat16).reshape(tokens_here, q_cols)
    projected = lax.psum_scatter(
        jnp.dot(attended, w_out, preferred_element_type=jnp.float32).astype(jnp.bfloat16),
        "tp",
        scatter_dimension=0,
        tiled=True,
    ).astype(jnp.float32)
    return (latent.astype(jnp.float32) + gate[0][None, :] * projected).astype(jnp.bfloat16)


def solution(mesh):
    in_specs = (
        P(("sp", "tp"), None),
        P("sp", None),
        P(),
        P(),
        P("sp", "tp"),
        P("sp", "tp"),
        P("sp", "tp"),
        P(None, "tp"),
        P(None, "tp"),
        P(None, "tp"),
        P("tp", None),
        P(),
    )
    out_specs = P(("sp", "tp"), None)
    return jax.shard_map(shards, mesh=mesh, in_specs=in_specs, out_specs=out_specs, check_vma=False)
```

profile of v0, /device:TPU:0, one launch (start us, length us, event | category | flops | bytes accessed | tf_op | source)
XLA Modules:
  0.0 259.0 jit_solution(11385487950224661711)
XLA Ops:
  11.9 38.9 %all-reduce = (f32[2,1024]{1,0:T(2,128)S(1)}, f32[2,1024]{1,0:T(2,128)S(1)}, f32[1,1024]{1,0:T(1,128)S(1)}) all-reduce(f32[2,1024]{1,0:T(2,128)S(1)} %fusion.55, f32[2,1024]{1,0:T(2,128)S(1)} %fusion.54, f32[1,1024]{1,0:T(1,128)S(1)} %fusion.42), channel_id=1, replica_groups=mesh['sp'=8,'tp'=4] {'sp'}, use_global_device_ids=true, to_apply=%region_4.5 | all-reduce | flops 5120 | bytes 40960 | tf_op jit(solution)/shard_map/psum | solution.py:95
  50.8 5.2 %all_gather.17 = f32[2,4096]{1,0:T(2,128)S(1)} all-gather(f32[2,1024]{1,0:T(2,128)S(1)} %get-tuple-element.5), channel_id=1, replica_groups=mesh['sp'=8,'tp'=4] {'tp'}, dimensions={1}, use_global_device_ids=true | all-gather | bytes 40960 | tf_op jit(solution)/shard_map/all_gather | solution.py:97
  56.0 5.2 %all_gather.16 = f32[2,4096]{1,0:T(2,128)S(1)} all-gather(f32[2,1024]{1,0:T(2,128)S(1)} %get-tuple-element.6), channel_id=1, replica_groups=mesh['sp'=8,'tp'=4] {'tp'}, dimensions={1}, use_global_device_ids=true | all-gather | bytes 40960 | tf_op jit(solution)/shard_map/all_gather | solution.py:98
  61.9 2.2 convolution_convert_fusion.4
  71.4 1.9 fusion.32
  73.4 29.7 %all-gather.5.cloned.1.call-done = bf16[1024,512]{1,0:T(8,128)(2,1)} async-done(((bf16[128,512]{1,0:T(8,128)(2,1)}), bf16[1024,512]{1,0:T(8,128)(2,1)}) %all-gather.5.cloned.1.call-update) | async-done | bytes 1048592 | tf_op jit(solution)/shard_map/all_gather | solution.py:105
  103.1 2.3 fusion.49
  105.3 2.0 copy.150
  107.4 2.0 reshape.310
  109.4 28.5 %all-gather.3.cloned.1.call-done = bf16[512,4096]{1,0:T(8,128)(2,1)} async-done(((bf16[128,4096]{1,0:T(8,128)(2,1)}), bf16[512,4096]{1,0:T(8,128)(2,1)}) %all-gather.3.cloned.1.call-update) | async-done | bytes 4194320 | tf_op jit(solution)/shard_map/all_gather | solution.py:121
  137.9 5.9 %convolution_convert_fusion.1 = bf16[512,512]{0,1:T(8,128)(2,1)S(1)} fusion(bf16[512,4096]{1,0:T(8,128)(2,1)} %all-gather.3.cloned.1.call-done, bf16[4096,512]{1,0:T(8,128)(2,1)} %param.19), kind=kOutput, calls=%fused_computation.33 | convolution fusion | flops 2147745792 | bytes 8912896 | tf_op jit(solution)/shard_map/dot_general | solution.py:124
  152.7 3.5 %convolution_convert_fusion.3 = bf16[512,256]{0,1:T(8,128)(2,1)S(1)} fusion(bf16[512,4096]{1,0:T(8,128)(2,1)} %all-gather.3.cloned.1.call-done, bf16[4096,256]{1,0:T(8,128)(2,1)S(1)} %copy-done), kind=kOutput, calls=%fused_computation.36 | convolution fusion | flops 1073872896 | bytes 6553600 | tf_op jit(solution)/shard_map/dot_general | solution.py:125
  157.3 1.7 multiply_subtract_fusion
  162.2 3.0 %convolution_convert_fusion.2 = bf16[512,256]{1,0:T(8,128)(2,1)S(1)} fusion(bf16[512,4096]{1,0:T(8,128)(2,1)S(1)} %copy-done.17, bf16[4096,256]{1,0:T(8,128)(2,1)} %param.21), kind=kOutput, calls=%fused_computation.35 | convolution fusion | flops 1073872896 | bytes 6553600 | tf_op jit(solution)/shard_map/dot_general | solution.py:126
  165.3 3.5 %collective-permute-start = (bf16[128,512]{1,0:T(8,128)(2,1)S(1)}, bf16[128,512]{1,0:T(8,128)(2,1)S(1)}, u32[]{:S(2)}, u32[]{:S(2)}) collective-permute-start(bf16[128,512]{1,0:T(8,128)(2,1)S(1)} %get-tuple-element.24), channel_id=1, source_target_pairs={{0,4},{4,8},{8,12},{12,16},{16,20},{20,24},{24,28},{1,5},{5,9},{9,... | collective-permute-start | bytes 393224 | tf_op jit(solution)/shard_map/ppermute | solution.py:22
  171.0 4.5 %fusion.52 = (f32[4,2,2,128]{3,2,0,1:T(2,128)S(1)}, f32[4,2,2,128,1024]{3,4,2,0,1:T(8,128)}) fusion(bf16[4,128,2,2,128]{4,1,3,2,0:T(8,128)(2,1)S(1)} %pad_maximum_fusion.5, bf16[1024,2,128,1,1]{2,1,0,4,3:T(2,128)(2,1)S(1)} %bitcast.86), kind=kOutput, calls=%fused_computation.104 | convolution fusion | flops 541063168 | bytes 9445376 | tf_op jit(solution)/shard_map/nqhgd,khd->nhgqk/dot_general | solution.py:185
  180.9 6.0 %fusion.1 = f32[4,2,2,128]{3,2,0,1:T(2,128)S(1)} fusion(f32[4,2,2,128,1024]{3,4,2,0,1:T(8,128)} %get-tuple-element.43, f32[4,2,2,128]{3,2,0,1:T(2,128)S(1)} %copy.132, f32[4,2,2,128,384]{3,4,2,1,0:T(8,128)S(1)} %get-tuple-element.45), kind=kLoop, calls=%fused_computation.4 | loop fusion | flops 8648704 | bytes 11550720 | tf_op jit(solution)/shard_map/reduce_sum | solution.py:67
  187.1 4.6 %divide_convert_fusion = bf16[4,2,2,128,1408]{3,4,2,0,1:T(8,128)(2,1)} fusion(f32[4,2,2,128,1024]{3,4,2,0,1:T(8,128)S(1)} %bitcast.78, f32[4,2,2,128]{3,2,0,1:T(2,128)S(1)} %copy.134, f32[4,2,2,128]{3,2,0,1:T(2,128)S(1)} %copy.132, f32[4,2,2,128,384]{3,4,2,1,0:T(8,128)S(1)} %get-tuple-element.45), kind=kLoop, calls=%fused_computation.2 | loop fusion | flops 11534336 | bytes 17317888 | tf_op jit(solution)/shard_map/convert_element_type | solution.py:67
  192.1 2.9 %fusion.22 = f32[4,128,2,2,128]{1,4,3,2,0:T(8,128)S(1)} fusion(bf16[1024,2,128,1,1]{0,2,4,1,3:T(8,128)(2,1)S(1)} %bitcast.90, bf16[4,2,2,128,1408]{3,4,2,0,1:T(8,128)(2,1)} %divide_convert_fusion), kind=kOutput, calls=%fused_computation.31 | convolution fusion | flops 536870912 | bytes 5767168 | tf_op jit(solution)/shard_map/nhgqk,khd->nqhgd/dot_general | solution.py:202
  195.0 1.9 fusion.28
  197.5 6.5 %convolution_convert_fusion = bf16[512,4096]{1,0:T(8,128)(2,1)} fusion(bf16[512,512]{1,0:T(8,128)(2,1)S(1)} %reshape.312, bf16[512,4096]{1,0:T(8,128)(2,1)} %param.22), kind=kOutput, calls=%fused_computation.5 | convolution fusion | flops 2149580800 | bytes 8912896 | tf_op jit(solution)/shard_map/dot_general | solution.py:210
  204.0 5.3 %all_gather.15 = f32[1,4096]{1,0:T(1,128)S(1)} all-gather(f32[1,1024]{1,0:T(1,128)S(1)} %get-tuple-element.7), channel_id=1, replica_groups=mesh['sp'=8,'tp'=4] {'tp'}, dimensions={1}, use_global_device_ids=true | all-gather | bytes 20480 | tf_op jit(solution)/shard_map/all_gather | solution.py:99
  209.4 40.6 %reduce-scatter.2.cloned.1.call-done = bf16[128,4096]{1,0:T(8,128)(2,1)} async-done(((bf16[512,4096]{1,0:T(8,128)(2,1)}), bf16[128,4096]{1,0:T(8,128)(2,1)}) %reduce-scatter.2.cloned.1.call-update) | async-done | bytes 1048592 | tf_op jit(solution)/shard_map/reduce_scatter | solution.py:209
  249.9 2.5 fusion.16
  (115 shorter events, 35.1 us)
Async XLA Ops:
  6.5 57.6 %copy-start = (bf16[4096,256]{1,0:T(8,128)(2,1)S(1)}, bf16[4096,256]{1,0:T(8,128)(2,1)}, u32[]{:S(2)}) copy-start(bf16[4096,256]{1,0:T(8,128)(2,1)} %param.20) | copy-start | bytes 6291460
  6.5 54.7 %copy-start.3 = (bf16[128,4096]{1,0:T(8,128)(2,1)S(1)}, bf16[128,4096]{1,0:T(8,128)(2,1)}, u32[]{:S(2)}) copy-start(bf16[128,4096]{1,0:T(8,128)(2,1)} %param.13) | copy-start | bytes 3145732
  6.5 96.6 %all-gather.5.cloned.1.call-start = ((), (), s32[]{:S(2)}) async-start(), calls=%async_computation.2 | async-start | bytes 1179648 | tf_op jit(solution)/shard_map/all_gather | solution.py:105
  61.5 2.6 %copy-start.4 = (bf16[128,4096]{1,0:T(8,128)(2,1)S(1)}, bf16[128,4096]{1,0:T(8,128)(2,1)}, u32[]{:S(2)}) copy-start(bf16[128,4096]{1,0:T(8,128)(2,1)} %param.13) | copy-start | bytes 3145732
  65.4 72.4 %all-gather.3.cloned.1.call-start = ((), (), s32[]{:S(2)}) async-start(), calls=%async_computation.1 | async-start | bytes 5242880 | tf_op jit(solution)/shard_map/all_gather | solution.py:121
  65.7 5.4 %copy-start.18 = (f32[16]{0:T(128)S(1)}, f32[16]{0:T(128)}, u32[]{:S(2)}) copy-start(f32[16]{0:T(128)} %param.23) | copy-start | bytes 196
  67.6 182.3 %reduce-scatter.2.cloned.1.call-start = ((), (), s32[]{:S(2)}) async-start(), calls=%async_computation.3 | async-start | bytes 5242880 | tf_op jit(solution)/shard_map/reduce_scatter | solution.py:209
  68.4 1.7 copy-start.12
  137.8 6.0 %copy-start.13 = (f32[512,32]{0,1:T(8,128)S(1)}, f32[512,32]{0,1:T(8,128)}, u32[]{:S(2)}) copy-start(f32[512,32]{0,1:T(8,128)} %copy-done.12) | copy-start | bytes 196612
  137.9 6.0 %copy-start.15 = (f32[512,32]{0,1:T(8,128)S(1)}, f32[512,32]{0,1:T(8,128)}, u32[]{:S(2)}) copy-start(f32[512,32]{0,1:T(8,128)} %copy-done.14) | copy-start | bytes 196612
  157.3 4.9 %copy-start.17 = (bf16[512,4096]{1,0:T(8,128)(2,1)S(1)}, bf16[512,4096]{1,0:T(8,128)(2,1)}, u32[]{:S(2)}) copy-start(bf16[512,4096]{1,0:T(8,128)(2,1)} %all-gather.3.cloned.1.call-done) | copy-start | bytes 12582916
  162.2 8.1 %copy-start.6 = (bf16[4,128,2,2,32]{4,1,3,2,0:T(8,128)(2,1)S(1)}, bf16[4,128,2,2,32]{4,1,3,2,0:T(8,128)(2,1)}, u32[]{:S(2)}) copy-start(bf16[4,128,2,2,32]{4,1,3,2,0:T(8,128)(2,1)} %copy.125) | copy-start | bytes 393220
  162.2 8.1 %copy-start.7 = (bf16[4,128,2,2,32]{4,1,3,2,0:T(8,128)(2,1)S(1)}, bf16[4,128,2,2,32]{4,1,3,2,0:T(8,128)(2,1)}, u32[]{:S(2)}) copy-start(bf16[4,128,2,2,32]{4,1,3,2,0:T(8,128)(2,1)} %copy.124) | copy-start | bytes 393220
  162.2 8.1 %copy-start.8 = (bf16[4,128,2,2,32]{4,1,3,2,0:T(8,128)(2,1)S(1)}, bf16[4,128,2,2,32]{4,1,3,2,0:T(8,128)(2,1)}, u32[]{:S(2)}) copy-start(bf16[4,128,2,2,32]{4,1,3,2,0:T(8,128)(2,1)} %copy.123) | copy-start | bytes 393220
  162.2 8.1 %copy-start.9 = (bf16[4,128,2,2,32]{4,1,3,2,0:T(8,128)(2,1)S(1)}, bf16[4,128,2,2,32]{4,1,3,2,0:T(8,128)(2,1)}, u32[]{:S(2)}) copy-start(bf16[4,128,2,2,32]{4,1,3,2,0:T(8,128)(2,1)} %copy.122) | copy-start | bytes 393220
  165.2 5.8 %copy-start.10 = (bf16[1024,2,128]{2,1,0:T(2,128)(2,1)S(1)}, bf16[1024,2,128]{2,1,0:T(2,128)(2,1)}, u32[]{:S(2)}) copy-start(bf16[1024,2,128]{2,1,0:T(2,128)(2,1)} %reshape.310) | copy-start | bytes 1572868
  165.3 10.5 %collective-permute-start = (bf16[128,512]{1,0:T(8,128)(2,1)S(1)}, bf16[128,512]{1,0:T(8,128)(2,1)S(1)}, u32[]{:S(2)}, u32[]{:S(2)}) collective-permute-start(bf16[128,512]{1,0:T(8,128)(2,1)S(1)} %get-tuple-element.24), channel_id=1, source_target_pairs={{0,4},{4,8},{8,12},{12,16},{16,20},{20,24},{24,28},{1,5},{5,9},{9,... | collective-permute-start | bytes 393224 | tf_op jit(solution)/shard_map/ppermute | solution.py:22
  168.8 7.4 %collective-permute-start.1 = (bf16[128,512]{1,0:T(8,128)(2,1)S(1)}, bf16[128,512]{1,0:T(8,128)(2,1)}, u32[]{:S(2)}, u32[]{:S(2)}) collective-permute-start(bf16[128,512]{1,0:T(8,128)(2,1)S(1)} %get-tuple-element.25), channel_id=1, source_target_pairs={{4,0},{8,4},{12,8},{16,12},{20,16},{24,20},{28,24},{5,1},{9,5},{13... | collective-permute-start | bytes 393224 | tf_op jit(solution)/shard_map/ppermute | solution.py:24
  177.2 2.8 %copy-start.11 = (pred[4,128,384]{1,2,0:T(8,128)(4,1)S(1)}, pred[4,128,384]{1,2,0:T(8,128)(4,1)}, u32[]{:S(2)}) copy-start(pred[4,128,384]{1,2,0:T(8,128)(4,1)} %fusion.32) | copy-start | bytes 589828
  180.1 6.9 %slice-start = ((s8[8388608]{0:T(1024)(128)(4,1)}), s8[4194304]{0:T(1024)(128)(4,1)S(1)}, s32[]{:S(2)}) async-start(s8[8388608]{0:T(1024)(128)(4,1)} %bitcast.77), calls=%async_computation.4 | async-start | bytes 8388608
  180.9 6.1 %slice-start.1 = ((s8[8388608]{0:T(1024)(128)(4,1)}), s8[4194304]{0:T(1024)(128)(4,1)S(1)}, s32[]{:S(2)}) async-start(s8[8388608]{0:T(1024)(128)(4,1)} %bitcast.77), calls=%async_computation.5 | async-start | bytes 8388608
  187.0 4.7 %copy-start.5 = (bf16[4,384,256]{2,1,0:T(8,128)(2,1)S(1)}, bf16[4,384,256]{2,1,0:T(8,128)(2,1)}, u32[]{:S(2)}) copy-start(bf16[4,384,256]{2,1,0:T(8,128)(2,1)} %get-tuple-element.8) | copy-start | bytes 2359300
  187.1 5.0 %copy-start.16 = (bf16[1024,256]{0,1:T(8,128)(2,1)S(1)}, bf16[1024,256]{0,1:T(8,128)(2,1)}, u32[]{:S(2)}) copy-start(bf16[1024,256]{0,1:T(8,128)(2,1)} %copy.150) | copy-start | bytes 1572868
  204.0 48.4 %copy-start.1 = (bf16[4096,256]{1,0:T(8,128)(2,1)S(1)}, bf16[4096,256]{1,0:T(8,128)(2,1)}, u32[]{:S(2)}) copy-start(bf16[4096,256]{1,0:T(8,128)(2,1)} %param.20) | copy-start | bytes 6291460
  (2 other events, 3.0 us)
Sparse Core Ops, SparseCore 0:
  65.5 37.5 all-gather.4
  104.6 33.1 all-gather.2
  204.2 45.7 reduce-scatter.1
where the time goes:
time: 260 us; the launch traced here: 259 us
  waiting for transfers between devices  99.3 us (38%)
  blocking collectives  54.6 us (21%)
  matrix products  36 us (14%)
  other arithmetic  28.1 us (11%)
  local copies, waits for them, and re-layouts  22.1 us (8%)
  between operations  13.6 us (5%)
  starting transfers between devices  5.29 us (2%)
    reduce_scatter x1, waiting for transfers between devices, shards(): lax.psum_scatter(jnp.dot(attended, w_out, preferred_element_type=jnp.floa...  40.6 us
    psum x1, blocking collectives, shards(): lax.psum((shift_part, scale_part, gate_part), 'sp')  38.9 us
    all_gather x1, waiting for transfers between devices, shards(): lax.all_gather(jnp.concatenate([jnp.dot(ctx_mod, key_weight, preferred_el...  29.7 us
    all_gather x1, waiting for transfers between devices, shards(): piece = lax.all_gather(latent_mod, 'tp', axis=0, tiled=True)  28.5 us
    concatenate x8, local copies, waits for them, and re-layouts, axial_rotation(): jnp.concatenate([rotate_half(values[..., :width], token_position // grid,...  7.91 us
    dot_general x1, matrix products, shards(): jnp.dot(attended, w_out, preferred_element_type=jnp.float32)  6.47 us
    reduce_sum x1, other arithmetic, sink_weights(): jnp.sum(expo, axis=-1, keepdims=True) + jnp.exp(sink_column - top)  6.03 us
    dot_general x1, matrix products, shards(): jnp.dot(piece, w_query, preferred_element_type=jnp.float32)  5.86 us
  transfers between devices with their start and end apart: 5, of which 4 were waited for; matrix products, arithmetic and copies ran while one was open for 7% of the time, Pallas kernels for 0%

commit v1 on v0

--- a/solution.py
+++ b/solution.py
@@ -9,6 +9,16 @@
 EPS = 1e-05
 THETA = 10000.0
 MASKED = -1e30
+
+
+def around_the_ring(array, axis, dim):
+    n_dev = lax.axis_size(axis)
+    held, shards = (array, [array])
+    for _ in range(n_dev - 1):
+        held = lax.ppermute(held, axis, [(i, (i + 1) % n_dev) for i in range(n_dev)])
+        shards.insert(0, held)
+    merged = jnp.concatenate(shards, axis=dim)
+    return jnp.roll(merged, (lax.axis_index(axis) + 1) * array.shape[dim], axis=dim)
 
 
 def with_halo(cells, sides, width):
@@ -118,7 +128,7 @@
         axis=0,
         tiled=True,
     )
-    piece = lax.all_gather(latent_mod, "tp", axis=0, tiled=True)
+    piece = around_the_ring(latent_mod, "tp", 0)
     projected_rows = jnp.concatenate(
         [
             jnp.dot(piece, w_query, preferred_element_type=jnp.float32).astype(jnp.bfloat16),

time: 260 us -> 252 us (0.969)
  waiting for transfers between devices: 99.3 us -> 84 us
  local copies, waits for them, and re-layouts: 22.1 us -> 32.3 us
  matrix products: 36 us -> 30.3 us
  other arithmetic: 28.1 us -> 31 us
    all_gather x1 -> x0, waiting for transfers between devices: 28.5 us -> none  [shards(): piece = lax.all_gather(latent_mod, 'tp', axis=0, tiled=True)]
    ppermute x0 -> x3, waiting for transfers between devices: none -> 21.3 us  [around_the_ring(): lax.ppermute(held, axis, [(i, (i + 1) % n_dev) for i in range(n_dev)])]
    unnamed x47, local copies, waits for them, and re-layouts: 1.07 us -> 12.4 us
    all_gather x1, waiting for transfers between devices: 29.7 us -> 22.3 us  [shards(): lax.all_gather(jnp.concatenate([jnp.dot(ctx_mod, key_weight, preferred_el...]
    concatenate x8, local copies, waits for them, and re-layouts: 7.91 us -> 4.6 us  [axial_rotation(): jnp.concatenate([rotate_half(values[..., :width], token_position // grid,...]
  transfers between devices with their start and end apart: 5 -> 7, of which waited for: 4 -> 4; matrix products, arithmetic and copies ran while one was open for 7% -> 13% of each run, Pallas kernels for 0% -> 0%
where the time goes in v1:
time: 252 us; the launch traced here: 251 us
  waiting for transfers between devices  84 us (33%)
  blocking collectives  54.7 us (22%)
  local copies, waits for them, and re-layouts  32.3 us (13%)
  other arithmetic  31 us (12%)
  matrix products  30.3 us (12%)
  between operations  13.9 us (6%)
  starting transfers between devices  5.2 us (2%)
    reduce_scatter x1, waiting for transfers between devices, shards(): lax.psum_scatter(jnp.dot(attended, w_out, preferred_element_type=jnp.floa...  40.5 us
    psum x1, blocking collectives, shards(): lax.psum((shift_part, scale_part, gate_part), 'sp')  38.9 us
    all_gather x1, waiting for transfers between devices, shards(): lax.all_gather(jnp.concatenate([jnp.dot(ctx_mod, key_weight, preferred_el...  22.3 us
    ppermute x3, waiting for transfers between devices, around_the_ring(): lax.ppermute(held, axis, [(i, (i + 1) % n_dev) for i in range(n_dev)])  21.3 us
    unnamed x47, local copies, waits for them, and re-layouts  12.4 us
    dot_general x1, matrix products, shards(): jnp.dot(attended, w_out, preferred_element_type=jnp.float32)  6.49 us
    reduce_sum x1, other arithmetic, sink_weights(): jnp.sum(expo, axis=-1, keepdims=True) + jnp.exp(sink_column - top)  6.03 us
    dot_general x1, matrix products, shards(): jnp.einsum('nqhgd,khd->nhgqk', query_block_list, context_key_rows, prefer...  5.54 us
  transfers between devices with their start and end apart: 7, of which 4 were waited for; matrix products, arithmetic and copies ran while one was open for 13% of the time, Pallas kernels for 0%

profile of v1, /device:TPU:0, one launch (start us, length us, event | category | flops | bytes accessed | tf_op | source)
XLA Modules:
  0.0 251.4 jit_solution(3164213883459555789)
XLA Ops:
  11.9 38.9 %all-reduce = (f32[2,1024]{1,0:T(2,128)S(1)}, f32[2,1024]{1,0:T(2,128)S(1)}, f32[1,1024]{1,0:T(1,128)S(1)}) all-reduce(f32[2,1024]{1,0:T(2,128)S(1)} %fusion.73, f32[2,1024]{1,0:T(2,128)S(1)} %fusion.72, f32[1,1024]{1,0:T(1,128)S(1)} %fusion.57), channel_id=1, replica_groups=mesh['sp'=8,'tp'=4] {'sp'}, use_global_device_ids=true, to_apply=%region_4.5 | all-reduce | flops 5120 | bytes 40960 | tf_op jit(solution)/shard_map/psum | solution.py:105
  50.8 5.3 %all_gather.13 = f32[2,4096]{1,0:T(2,128)S(1)} all-gather(f32[2,1024]{1,0:T(2,128)S(1)} %get-tuple-element.6), channel_id=1, replica_groups=mesh['sp'=8,'tp'=4] {'tp'}, dimensions={1}, use_global_device_ids=true | all-gather | bytes 40960 | tf_op jit(solution)/shard_map/all_gather | solution.py:108
  56.2 5.2 %all_gather.14 = f32[2,4096]{1,0:T(2,128)S(1)} all-gather(f32[2,1024]{1,0:T(2,128)S(1)} %get-tuple-element.5), channel_id=1, replica_groups=mesh['sp'=8,'tp'=4] {'tp'}, dimensions={1}, use_global_device_ids=true | all-gather | bytes 40960 | tf_op jit(solution)/shard_map/all_gather | solution.py:107
  65.4 11.6 %collective-permute-done = bf16[128,4096]{1,0:T(8,128)(2,1)} collective-permute-done((bf16[128,4096]{1,0:T(8,128)(2,1)S(1)}, bf16[128,4096]{1,0:T(8,128)(2,1)}, u32[]{:S(2)}, u32[]{:S(2)}) %collective-permute-start) | collective-permute-done | bytes 1048608 | tf_op jit(solution)/shard_map/ppermute | solution.py:18
  81.8 9.7 %collective-permute-done.1 = bf16[128,4096]{1,0:T(8,128)(2,1)} collective-permute-done((bf16[128,4096]{1,0:T(8,128)(2,1)}, bf16[128,4096]{1,0:T(8,128)(2,1)}, u32[]{:S(2)}, u32[]{:S(2)}) %collective-permute-start.1) | collective-permute-done | bytes 1048608 | tf_op jit(solution)/shard_map/ppermute | solution.py:18
  91.6 1.9 fusion.47
  93.5 22.3 %all-gather.2.cloned.1.call-done = bf16[1024,512]{1,0:T(8,128)(2,1)} async-done(((bf16[128,512]{1,0:T(8,128)(2,1)}), bf16[1024,512]{1,0:T(8,128)(2,1)}) %all-gather.2.cloned.1.call-update) | async-done | bytes 1048592 | tf_op jit(solution)/shard_map/all_gather | solution.py:115
  115.8 2.2 fusion.67
  118.1 2.0 reshape.310
  120.1 2.0 copy.150
  132.3 2.2 copy-done.11
  138.3 1.7 multiply_subtract_fusion.1
  144.0 3.1 %collective-permute-start.3 = (bf16[128,512]{1,0:T(8,128)(2,1)}, bf16[128,512]{1,0:T(8,128)(2,1)}, u32[]{:S(2)}, u32[]{:S(2)}) collective-permute-start(bf16[128,512]{1,0:T(8,128)(2,1)} %get-tuple-element.24), channel_id=1, source_target_pairs={{0,4},{4,8},{8,12},{12,16},{16,20},{20,24},{24,28},{1,5},{5,9},{9,... | collective-permute-start | bytes 393224 | tf_op jit(solution)/shard_map/ppermute | solution.py:32
  148.8 4.6 %fusion.34 = bf16[512,512]{0,1:T(8,128)(2,1)S(1)} fusion(bf16[4096,512]{1,0:T(8,128)(2,1)S(1)} %copy-done.12, bf16[1024,4096]{1,0:T(8,128)(2,1)} %copy-done.11, s32[]{:T(128)S(6)} %select_n.47), kind=kOutput, calls=%fused_computation.39 | convolution fusion | flops 2147745792 | bytes 8912900 | tf_op jit(solution)/shard_map/dot_general | solution.py:134
  159.0 1.9 pad_maximum_fusion.5
  160.9 5.5 %fusion.70 = (f32[4,2,2,128]{3,2,0,1:T(2,128)S(1)}, f32[4,2,2,128,1024]{3,4,2,0,1:T(8,128)}) fusion(bf16[4,128,2,2,128]{4,1,3,2,0:T(8,128)(2,1)S(1)} %pad_maximum_fusion.5, bf16[1024,2,128,1,1]{2,1,0,4,3:T(2,128)(2,1)} %bitcast.83), kind=kOutput, calls=%fused_computation.121 | convolution fusion | flops 541063168 | bytes 9445376 | tf_op jit(solution)/shard_map/nqhgd,khd->nhgqk/dot_general | solution.py:195
  173.1 6.0 %fusion.1 = f32[4,2,2,128]{3,2,0,1:T(2,128)S(1)} fusion(f32[4,2,2,128,1024]{3,4,2,0,1:T(8,128)} %get-tuple-element.43, f32[4,2,2,128]{3,2,0,1:T(2,128)S(1)} %copy.132, f32[4,2,2,128,384]{3,4,2,1,0:T(8,128)S(1)} %get-tuple-element.45), kind=kLoop, calls=%fused_computation.4 | loop fusion | flops 8648704 | bytes 11550720 | tf_op jit(solution)/shard_map/reduce_sum | solution.py:77
  179.3 4.6 %divide_convert_fusion = bf16[4,2,2,128,1408]{3,4,2,0,1:T(8,128)(2,1)} fusion(f32[4,2,2,128,1024]{3,4,2,0,1:T(8,128)S(1)} %bitcast.75, f32[4,2,2,128]{3,2,0,1:T(2,128)S(1)} %copy.134, f32[4,2,2,128]{3,2,0,1:T(2,128)S(1)} %copy.132, f32[4,2,2,128,384]{3,4,2,1,0:T(8,128)S(1)} %get-tuple-element.45), kind=kLoop, calls=%fused_computation.2 | loop fusion | flops 11534336 | bytes 17317888 | tf_op jit(solution)/shard_map/convert_element_type | solution.py:77
  184.3 2.9 %fusion.28 = f32[4,128,2,2,128]{1,4,3,2,0:T(8,128)S(1)} fusion(bf16[1024,2,128,1,1]{0,2,4,1,3:T(8,128)(2,1)S(1)} %bitcast.87, bf16[4,2,2,128,1408]{3,4,2,0,1:T(8,128)(2,1)} %divide_convert_fusion), kind=kOutput, calls=%fused_computation.37 | convolution fusion | flops 536870912 | bytes 5767168 | tf_op jit(solution)/shard_map/nhgqk,khd->nqhgd/dot_general | solution.py:212
  187.2 1.9 fusion.37
  189.7 6.5 %convolution_convert_fusion = bf16[512,4096]{1,0:T(8,128)(2,1)} fusion(bf16[512,512]{1,0:T(8,128)(2,1)S(1)} %reshape.312, bf16[512,4096]{1,0:T(8,128)(2,1)} %param.22), kind=kOutput, calls=%fused_computation.5 | convolution fusion | flops 2149580800 | bytes 8912896 | tf_op jit(solution)/shard_map/dot_general | solution.py:220
  196.2 5.3 %all_gather.12 = f32[1,4096]{1,0:T(1,128)S(1)} all-gather(f32[1,1024]{1,0:T(1,128)S(1)} %get-tuple-element.7), channel_id=1, replica_groups=mesh['sp'=8,'tp'=4] {'tp'}, dimensions={1}, use_global_device_ids=true | all-gather | bytes 20480 | tf_op jit(solution)/shard_map/all_gather | solution.py:109
  201.6 40.5 %reduce-scatter.2.cloned.1.call-done = bf16[128,4096]{1,0:T(8,128)(2,1)} async-done(((bf16[512,4096]{1,0:T(8,128)(2,1)}), bf16[128,4096]{1,0:T(8,128)(2,1)}) %reduce-scatter.2.cloned.1.call-update) | async-done | bytes 1048592 | tf_op jit(solution)/shard_map/reduce_scatter | solution.py:219
  242.0 2.5 fusion.22
  (120 shorter events, 47.1 us)
Async XLA Ops:
  6.5 57.1 %copy-start = (bf16[4096,256]{1,0:T(8,128)(2,1)S(1)}, bf16[4096,256]{1,0:T(8,128)(2,1)}, u32[]{:S(2)}) copy-start(bf16[4096,256]{1,0:T(8,128)(2,1)} %param.20) | copy-start | bytes 6291460
  6.5 54.8 %copy-start.2 = (bf16[128,4096]{1,0:T(8,128)(2,1)S(1)}, bf16[128,4096]{1,0:T(8,128)(2,1)}, u32[]{:S(2)}) copy-start(bf16[128,4096]{1,0:T(8,128)(2,1)} %param.12) | copy-start | bytes 3145732
  6.5 109.3 %all-gather.2.cloned.1.call-start = ((), (), s32[]{:S(2)}) async-start(), calls=%async_computation.1 | async-start | bytes 1179648 | tf_op jit(solution)/shard_map/all_gather | solution.py:115
  50.8 12.1 %copy-start.3 = (bf16[128,4096]{1,0:T(8,128)(2,1)S(1)}, bf16[128,4096]{1,0:T(8,128)(2,1)}, u32[]{:S(2)}) copy-start(bf16[128,4096]{1,0:T(8,128)(2,1)} %param.13) | copy-start | bytes 3145732
  62.6 14.4 %collective-permute-start = (bf16[128,4096]{1,0:T(8,128)(2,1)S(1)}, bf16[128,4096]{1,0:T(8,128)(2,1)}, u32[]{:S(2)}, u32[]{:S(2)}) collective-permute-start(bf16[128,4096]{1,0:T(8,128)(2,1)S(1)} %fusion.17), channel_id=1, source_target_pairs={{0,1},{1,2},{2,3},{3,0},{4,5},{5,6},{6,7},{7,4},{8,9},{9,10},{10,1... | collective-permute-start | bytes 3145736 | tf_op jit(solution)/shard_map/ppermute | solution.py:18
  64.8 16.9 %copy-start.15 = (f32[16]{0:T(128)S(1)}, f32[16]{0:T(128)}, u32[]{:S(2)}) copy-start(f32[16]{0:T(128)} %param.23) | copy-start | bytes 196
  76.9 14.5 %collective-permute-start.1 = (bf16[128,4096]{1,0:T(8,128)(2,1)}, bf16[128,4096]{1,0:T(8,128)(2,1)}, u32[]{:S(2)}, u32[]{:S(2)}) collective-permute-start(bf16[128,4096]{1,0:T(8,128)(2,1)} %collective-permute-done), channel_id=1, source_target_pairs={{0,1},{1,2},{2,3},{3,0},{4,5},{5,6},{6,7},{7,4},{8,9},{9,10},{10,1... | collective-permute-start | bytes 3145736 | tf_op jit(solution)/shard_map/ppermute | solution.py:18
  77.6 164.4 %reduce-scatter.2.cloned.1.call-start = ((), (), s32[]{:S(2)}) async-start(), calls=%async_computation.2 | async-start | bytes 5242880 | tf_op jit(solution)/shard_map/reduce_scatter | solution.py:219
  78.3 45.2 %copy-start.6 = (f32[512,32]{0,1:T(8,128)}, f32[512,32]{0,1:T(8,128)S(1)}, u32[]{:S(2)}) copy-start(f32[512,32]{0,1:T(8,128)S(1)} %get-tuple-element.40) | copy-start | bytes 196612
  78.3 45.2 %copy-start.8 = (f32[512,32]{0,1:T(8,128)}, f32[512,32]{0,1:T(8,128)S(1)}, u32[]{:S(2)}) copy-start(f32[512,32]{0,1:T(8,128)S(1)} %get-tuple-element.41) | copy-start | bytes 196612
  91.5 30.6 %collective-permute-start.2 = (bf16[128,4096]{1,0:T(8,128)(2,1)}, bf16[128,4096]{1,0:T(8,128)(2,1)}, u32[]{:S(2)}, u32[]{:S(2)}) collective-permute-start(bf16[128,4096]{1,0:T(8,128)(2,1)} %collective-permute-done.1), channel_id=1, source_target_pairs={{0,1},{1,2},{2,3},{3,0},{4,5},{5,6},{6,7},{7,4},{8,9},{9,10},{10,1... | collective-permute-start | bytes 3145736 | tf_op jit(solution)/shard_map/ppermute | solution.py:18
  130.9 3.5 %copy-start.11 = (bf16[1024,4096]{1,0:T(8,128)(2,1)}, bf16[1024,4096]{1,0:T(8,128)(2,1)S(1)}, u32[]{:S(2)}) copy-start(bf16[1024,4096]{1,0:T(8,128)(2,1)S(1)} %constant_dynamic-update-slice_fusion) | copy-start | bytes 25165828
  130.9 3.5 %copy-start.14 = (bf16[4096,256]{1,0:T(8,128)(2,1)S(1)}, bf16[4096,256]{1,0:T(8,128)(2,1)}, u32[]{:S(2)}) copy-start(bf16[4096,256]{1,0:T(8,128)(2,1)} %param.21) | copy-start | bytes 6291460
  138.3 10.5 %copy-start.12 = (bf16[4096,512]{1,0:T(8,128)(2,1)S(1)}, bf16[4096,512]{1,0:T(8,128)(2,1)}, u32[]{:S(2)}) copy-start(bf16[4096,512]{1,0:T(8,128)(2,1)} %param.19) | copy-start | bytes 12582916
  144.0 23.3 %collective-permute-start.3 = (bf16[128,512]{1,0:T(8,128)(2,1)}, bf16[128,512]{1,0:T(8,128)(2,1)}, u32[]{:S(2)}, u32[]{:S(2)}) collective-permute-start(bf16[128,512]{1,0:T(8,128)(2,1)} %get-tuple-element.24), channel_id=1, source_target_pairs={{0,4},{4,8},{8,12},{12,16},{16,20},{20,24},{24,28},{1,5},{5,9},{9,... | collective-permute-start | bytes 393224 | tf_op jit(solution)/shard_map/ppermute | solution.py:32
  147.1 6.4 %copy-start.7 = (f32[512,32]{0,1:T(8,128)S(1)}, f32[512,32]{0,1:T(8,128)}, u32[]{:S(2)}) copy-start(f32[512,32]{0,1:T(8,128)} %copy-done.6) | copy-start | bytes 196612
  147.1 6.4 %copy-start.9 = (f32[512,32]{0,1:T(8,128)S(1)}, f32[512,32]{0,1:T(8,128)}, u32[]{:S(2)}) copy-start(f32[512,32]{0,1:T(8,128)} %copy-done.8) | copy-start | bytes 196612
  147.1 20.2 %collective-permute-start.4 = (bf16[128,512]{1,0:T(8,128)(2,1)}, bf16[128,512]{1,0:T(8,128)(2,1)}, u32[]{:S(2)}, u32[]{:S(2)}) collective-permute-start(bf16[128,512]{1,0:T(8,128)(2,1)} %get-tuple-element.25), channel_id=1, source_target_pairs={{4,0},{8,4},{12,8},{16,12},{20,16},{24,20},{28,24},{5,1},{9,5},{13... | collective-permute-start | bytes 393224 | tf_op jit(solution)/shard_map/ppermute | solution.py:34
  169.5 2.8 %copy-start.5 = (pred[4,128,384]{1,2,0:T(8,128)(4,1)S(1)}, pred[4,128,384]{1,2,0:T(8,128)(4,1)}, u32[]{:S(2)}) copy-start(pred[4,128,384]{1,2,0:T(8,128)(4,1)} %fusion.47) | copy-start | bytes 589828
  172.3 6.9 %slice-start = ((s8[8388608]{0:T(1024)(128)(4,1)}), s8[4194304]{0:T(1024)(128)(4,1)S(1)}, s32[]{:S(2)}) async-start(s8[8388608]{0:T(1024)(128)(4,1)} %bitcast.74), calls=%async_computation.3 | async-start | bytes 8388608
  173.1 6.1 %slice-start.1 = ((s8[8388608]{0:T(1024)(128)(4,1)}), s8[4194304]{0:T(1024)(128)(4,1)S(1)}, s32[]{:S(2)}) async-start(s8[8388608]{0:T(1024)(128)(4,1)} %bitcast.74), calls=%async_computation.4 | async-start | bytes 8388608
  179.3 4.6 %copy-start.4 = (bf16[4,384,256]{2,1,0:T(8,128)(2,1)S(1)}, bf16[4,384,256]{2,1,0:T(8,128)(2,1)}, u32[]{:S(2)}) copy-start(bf16[4,384,256]{2,1,0:T(8,128)(2,1)} %get-tuple-element.8) | copy-start | bytes 2359300
  179.3 5.0 %copy-start.10 = (bf16[1024,256]{0,1:T(8,128)(2,1)S(1)}, bf16[1024,256]{0,1:T(8,128)(2,1)}, u32[]{:S(2)}) copy-start(bf16[1024,256]{0,1:T(8,128)(2,1)} %copy.150) | copy-start | bytes 1572868
  196.2 48.3 %copy-start.1 = (bf16[4096,256]{1,0:T(8,128)(2,1)S(1)}, bf16[4096,256]{1,0:T(8,128)(2,1)}, u32[]{:S(2)}) copy-start(bf16[4096,256]{1,0:T(8,128)(2,1)} %param.20) | copy-start | bytes 6291460
  (1 other events, 1.6 us)
Sparse Core Ops, SparseCore 0:
  77.8 38.0 all-gather.1
  196.4 45.6 reduce-scatter.1
